TPU v7x, 512 devices: a whole 4x4x16 slice. The times are simulated.
512 devices in a mesh: sp: 32 (over z, core), tp: 16 (over y, x).
Axes of the slice: x: 4, y: 4, z: 16, core: 2. Of those that a mesh axis runs over, the one named last changes fastest.
Arguments:
- query_rows: bfloat16 [8192, 2048], P('sp', 'tp'), may hold values from -1000 to 1000
- key_rows: bfloat16 [8192, 256], P('sp'), may hold values from -6 to 6
- value_rows: bfloat16 [8192, 256], P('sp'), may hold values from -6 to 6
- sink_logits: float32 [32], P('tp'), may hold values from 1 to 6
- out_weight: bfloat16 [2048, 2048], P('tp'), may hold values from -0.375 to 0.375
- stream_in: bfloat16 [8192, 2048], P('sp'), may hold values from -6 to 6
- norm_gain: float32 [2048], replicated, may hold values from 0.1 to 1.9
- routes: int32 [8192, 2], P('sp'), may hold values from 0 to 31, all different within a row; in each aligned block of 256 rows (0 to 255, 256 to 511, ...) at most 24 rows name the same one
- route_weights: float32 [8192, 2], P('sp'), may hold values from 0.2 to 1
- gate_weight: bfloat16 [32, 2048, 4096], P('sp', None, 'tp'), may hold values from -0.125 to 0.125
- up_weight: bfloat16 [32, 2048, 4096], P('sp', None, 'tp'), may hold values from -0.125 to 0.125
- down_weight: bfloat16 [32, 4096, 2048], P('sp', 'tp'), may hold values from -0.09375 to 0.09375
Outputs:
- layer_out: bfloat16 [8192, 2048], P(('sp', 'tp'))
Inputs may be any that keep to these rules, and one draw needn't show every extreme that they name: `routes`: each row names 2 different experts. Within the rows of one device (256 aligned rows) no expert is named more than 24 times, a bound that some block reaches.
All inputs are finite; a program needn't handle non-finite values.
Results may differ from a plain program's by a relative error of at most 0.015.
Values may be sent and summed in bfloat16 or wider, within the bound.
No kernel may reach another device: no remote copies, remote signals or barrier semaphores. Data moves between devices by JAX's collectives and lax.ppermute only.
A program may use at most 64 MiB of HBM per device.

v0:
```python
import jax
import jax.numpy as jnp
from jax import lax
from jax.sharding import Mesh
from jax.sharding import PartitionSpec as P

HEAD_DIM = 64
REP = 8
WINDOW = 128
TP = ("tp_0", "tp_1")
SP_TP = ("sp", "tp_0", "tp_1")
norm_eps = 1e-06


def shifted(block, axis, distance):
    devices = range(lax.axis_size(axis))
    route = [(i - distance, i) for i in devices if i - distance in devices]
    return lax.ppermute(block, axis, route)


def cut_along(shard, dim, count):
    before, after = (shard.shape[:dim], shard.shape[dim + 1 :])
    return jnp.moveaxis(shard.reshape(*before, count, -1, *after), dim, 0)


def sum_at_owner(shard, axis, dim):
    pieces = cut_along(shard, dim, lax.axis_size(axis))
    arrived = lax.all_to_all(pieces, axis, split_axis=0, concat_axis=0, tiled=True)
    return arrived.astype(jnp.float32).sum(axis=0)


def laid_out(pieces, dim):
    lengths = list(pieces.shape[1:])
    lengths[dim] *= pieces.shape[0]
    return jnp.moveaxis(pieces, 0, dim).reshape(lengths)


def sent_to_all(shard, axis):
    copies = jnp.broadcast_to(shard, (lax.axis_size(axis), *shard.shape))
    return lax.all_to_all(copies, axis, split_axis=0, concat_axis=0, tiled=True)


def gathered_copies(shard, axis, dim):
    return laid_out(sent_to_all(shard, axis), dim)


def gathered_by_axis(shard, axes, dim):
    result = shard
    for number in range(len(axes) - 1, -1, -1):
        result = lax.all_gather(result, axes[number], axis=dim, tiled=True)
    return result


def piece_ends(length, count):
    hop = length // count
    if hop >= 8:
        hop -= hop % 8
    return [hop * k for k in range(1, count)]


def exchange_in_pieces(shard, axis, pieces, split_dim, concat_dim):
    blocks = cut_along(shard, split_dim, lax.axis_size(axis))
    split_at = max(range(1, max(2, blocks.ndim - 1)), key=lambda d: blocks.shape[d])
    finished = []
    for slab in jnp.split(blocks, piece_ends(blocks.shape[split_at], pieces), axis=split_at):
        if slab.size:
            finished.append(lax.all_to_all(slab, axis, split_axis=0, concat_axis=0, tiled=True))
    return laid_out(jnp.concatenate(finished, axis=split_at), concat_dim)


def rms_scale(stream, norm_gain):
    values = stream.astype(jnp.float32)
    scaled = values * lax.rsqrt(jnp.mean(values * values, axis=-1, keepdims=True) + norm_eps)
    return (scaled * norm_gain).astype(jnp.bfloat16)


def slot_tables(routes, experts_n, slot_cap):
    flat_ids = routes.reshape(-1)
    onehot = (flat_ids[:, None] == jnp.arange(experts_n, dtype=jnp.int32)[None, :]).astype(
        jnp.int32
    )
    before = jnp.cumsum(onehot, axis=0) - onehot
    targets = flat_ids * slot_cap + jnp.sum(before * onehot, axis=1)
    pair_token = jnp.arange(flat_ids.shape[0], dtype=jnp.int32) // routes.shape[1]
    slot_token = jnp.zeros((experts_n * slot_cap,), jnp.int32).at[targets].set(pair_token)
    slot_live = jnp.zeros((experts_n * slot_cap,), jnp.int32).at[targets].set(1)
    return (targets, slot_token, slot_live)


def per_device(
    query_rows,
    key_rows,
    value_rows,
    sink_logits,
    out_weight,
    stream_in,
    norm_gain,
    routes,
    route_weights,
    gate_weight,
    up_weight,
    down_weight,
):
    tok_count = query_rows.shape[0]
    local_heads = query_rows.shape[1] // HEAD_DIM
    tp_index = lax.axis_index(TP)
    kv_group = tp_index * local_heads // REP
    own_keys = lax.dynamic_slice_in_dim(key_rows, kv_group * HEAD_DIM, HEAD_DIM, 1)
    own_values = lax.dynamic_slice_in_dim(value_rows, kv_group * HEAD_DIM, HEAD_DIM, 1)
    prior_keys, prior_values = shifted(
        (own_keys[tok_count - WINDOW :], own_values[tok_count - WINDOW :]), "sp", 1
    )
    key_block = jnp.concatenate([prior_keys, own_keys], axis=0)
    value_block = jnp.concatenate([prior_values, own_values], axis=0)
    offset = lax.axis_index("sp") * tok_count
    query_pos = offset + jnp.arange(tok_count, dtype=jnp.int32)
    key_pos = offset - WINDOW + jnp.arange(tok_count + WINDOW, dtype=jnp.int32)
    distance = query_pos[:, None] - key_pos[None, :]
    allowed = (distance >= 0) & (distance < WINDOW) & (key_pos >= 0)[None, :]
    queries = query_rows.reshape(tok_count, local_heads, HEAD_DIM)
    scores = jnp.einsum(
        "qhd,kd->hqk", queries, key_block, preferred_element_type=jnp.float32
    ) * HEAD_DIM ** (-0.5)
    scores = jnp.where(allowed[None], scores, -1e30)
    sink_col = sink_logits.reshape(local_heads, 1, 1)
    row_peak = jnp.maximum(jnp.max(scores, axis=-1, keepdims=True), sink_col)
    exp_terms = jnp.exp(scores - row_peak)
    denom_sum = jnp.sum(exp_terms, axis=-1, keepdims=True) + jnp.exp(sink_col - row_peak)
    attn_probs = (exp_terms / denom_sum).astype(jnp.bfloat16)
    attended = jnp.einsum(
        "hqk,kd->qhd", attn_probs, value_block, preferred_element_type=jnp.float32
    )
    attended = attended.astype(jnp.bfloat16).reshape(tok_count, local_heads * HEAD_DIM)
    width = out_weight.shape[1]
    width_share = width // lax.axis_size(TP)
    projected = sum_at_owner(
        jnp.dot(attended, out_weight, preferred_element_type=jnp.float32).astype(jnp.bfloat16),
        TP,
        1,
    )
    own_input = lax.dynamic_slice_in_dim(stream_in, tp_index * width_share, width_share, 1)
    columns = (own_input.astype(jnp.float32) + projected).astype(jnp.bfloat16)
    experts_n = lax.axis_size("sp")
    top_count = routes.shape[1]
    slot_cap = 3 * tok_count * top_count // (2 * experts_n)
    targets, slot_token, slot_live = slot_tables(routes, experts_n, slot_cap)
    outgoing = jnp.where(slot_live[:, None] > 0, columns[slot_token], jnp.zeros((), jnp.bfloat16))
    outgoing = outgoing.reshape(experts_n, slot_cap, width_share)
    arrived = lax.all_to_all(outgoing, "sp", split_axis=0, concat_axis=0, tiled=True)
    arrived = rms_scale(gathered_copies(arrived, TP, 2), norm_gain)
    sources = arrived.shape[0]
    item_count = arrived.shape[1]
    flat_rows = arrived.reshape(sources * item_count, arrived.shape[2])
    gate_act = jnp.dot(flat_rows, gate_weight[0], preferred_element_type=jnp.float32)
    up_act = jnp.dot(flat_rows, up_weight[0], preferred_element_type=jnp.float32)
    hidden = (jax.nn.silu(gate_act) * up_act).astype(jnp.bfloat16)
    partial_value = jnp.dot(hidden, down_weight[0], preferred_element_type=jnp.float32).astype(
        jnp.bfloat16
    )
    pieces = exchange_in_pieces(partial_value[None], TP, 1, 2, 0)
    summed = jnp.sum(pieces.astype(jnp.float32), axis=0)
    summed = summed.reshape(sources, item_count, summed.shape[1])
    returned = lax.all_to_all(
        summed.astype(jnp.bfloat16), "sp", split_axis=0, concat_axis=0, tiled=True
    ).astype(summed.dtype)
    returned_flat = returned.reshape(experts_n * slot_cap, returned.shape[2])
    pair_weights = route_weights.reshape(-1)
    chosen = returned_flat[targets] * pair_weights[:, None]
    moe_columns = jnp.sum(chosen.reshape(tok_count, top_count, chosen.shape[1]), axis=1)
    out_columns = (columns.astype(jnp.float32) + moe_columns).astype(jnp.bfloat16)
    return lax.all_to_all(out_columns, TP, split_axis=0, concat_axis=1, tiled=True)


def solution(mesh):
    finer = Mesh(mesh.devices.reshape(mesh.shape["sp"], 4, 4), ("sp", "tp_0", "tp_1"))
    placed = (
        P("sp", TP),
        P("sp", None),
        P("sp", None),
        P(TP),
        P(TP, None),
        P("sp", None),
        P(),
        P("sp", None),
        P("sp", None),
        P("sp", None, TP),
        P("sp", None, TP),
        P("sp", TP, None),
    )
    return jax.shard_map(
        per_device, mesh=finer, in_specs=placed, out_specs=P(SP_TP, None), check_vma=False
    )
```

profile of v0, /device:TPU:2, one launch (start us, length us, event | category | flops | bytes accessed | tf_op | source)
XLA Modules:
  0.0 221.7 jit_solution(14790796120273187725)
XLA Ops:
  0.0 0.0 copy-start
  0.0 1.0 constant_dynamic-slice_fusion
  1.0 0.1 copy.44
  1.1 1.7 collective-permute-start.1
  2.9 0.9 constant_dynamic-slice_fusion.1
  3.8 0.1 copy.43
  3.9 0.0 copy-start.2
  3.9 4.2 %collective-permute-start = (bf16[128,64]{0,1:T(8,128)(2,1)S(1)}, bf16[128,64]{0,1:T(8,128)(2,1)S(1)}, u32[]{:S(2)}, u32[]{:S(2)}) collective-permute-start(bf16[128,64]{0,1:T(8,128)(2,1)S(1)} %slice.20), channel_id=1, source_target_pairs={{0,16},{16,32},{32,48},{48,64},{64,80},{80,96},{96,112},{112,128},... | collective-permute-start | bytes 49160 | tf_op jit(solution)/shard_map/ppermute | solution.py:18
  8.2 0.8 copy.35
  9.1 0.7 broadcast_multiply_fusion
  9.7 0.1 eq.29
  9.9 1.2 reduce-window.6
  11.1 0.2 fusion.30
  11.3 0.2 slice_reduce_fusion
  11.5 0.1 eq.25
  11.6 0.9 copy.31
  12.6 0.1 copy.34
  12.7 0.1 mul.101
  12.9 0.0 collective-permute-done.1
  12.9 0.3 fusion.49
  13.2 0.7 broadcast_maximum_fusion
  13.9 0.1 fusion.27
  14.1 0.0 copy-done.5
  14.1 0.1 exponential_add_fusion
  14.1 0.0 collective-permute-done
  14.2 0.3 convolution_convert_fusion.2
  14.4 0.0 copy-done.2
  14.4 0.4 fusion.11
  14.9 1.3 copy.69
  16.2 7.5 %all-to-all-start = ((bf16[16,256,128]{2,1,0:T(8,128)(2,1)}), bf16[16,256,128]{2,1,0:T(8,128)(2,1)S(1)}, u32[]{:S(2)}, u32[]{:S(2)}) async-start(bf16[16,256,128]{2,1,0:T(8,128)(2,1)} %bitcast.94), calls=%async_computation | async-start | bytes 2097152 | tf_op jit(solution)/shard_map/all_to_all | solution.py:28
  23.6 0.1 fusion.33
  23.8 2.4 %scatter_custom_fusion.1 = s32[768]{0:T(1024)S(1)} fusion(s32[512]{0:T(512)S(1)} %bitcast.105, s32[512]{0:T(512)S(1)} %add_select_fusion, s32[]{:T(128)} %constant.30.clone.1), kind=kCustom, calls=%fused_computation.72 | custom fusion | bytes 3076 | tf_op jit(solution)/shard_map/scatter | solution.py:85
  26.2 2.4 %scatter_custom_fusion = s32[768]{0:T(1024)S(1)} fusion(s32[512]{0:T(512)S(1)} %bitcast.106, s32[512]{0:T(512)S(1)} %broadcast.197, s32[]{:T(128)} %constant.30.clone.1), kind=kCustom, calls=%fused_computation.75 | custom fusion | bytes 3076 | tf_op jit(solution)/shard_map/scatter | solution.py:86
  28.7 0.1 broadcast_in_dim.51
  28.8 10.8 %all-to-all-done = bf16[16,256,128]{2,1,0:T(8,128)(2,1)S(1)} async-done(((bf16[16,256,128]{2,1,0:T(8,128)(2,1)}), bf16[16,256,128]{2,1,0:T(8,128)(2,1)S(1)}, u32[]{:S(2)}, u32[]{:S(2)}) %all-to-all-start) | async-done | bytes 1048608 | tf_op jit(solution)/shard_map/all_to_all | solution.py:28
  39.6 0.1 convert_reduce_fusion
  39.7 0.9 add_convert_fusion.1
  40.6 1.9 gather_fusion
  42.5 0.2 broadcast_select_fusion
  42.7 34.4 %all_to_all.44 = bf16[32,24,128]{2,1,0:T(8,128)(2,1)S(1)} all-to-all(bf16[32,24,128]{2,1,0:T(8,128)(2,1)S(1)} %broadcast_select_fusion), channel_id=1, replica_groups=mesh['sp'=32,'tp_0'=4,'tp_1'=4] {'sp'}, dimensions={0} | all-to-all | bytes 393216 | tf_op jit(solution)/shard_map/all_to_all | solution.py:149
  77.1 0.6 broadcast_in_dim.55
  77.7 42.4 %all_to_all.45 = bf16[16,32,24,128]{3,2,1,0:T(8,128)(2,1)S(1)} all-to-all(bf16[16,32,24,128]{3,2,1,0:T(8,128)(2,1)S(1)} %broadcast_in_dim.55), channel_id=1, replica_groups=mesh['sp'=32,'tp_0'=4,'tp_1'=4] {'tp_0','tp_1'}, dimensions={0} | all-to-all | bytes 6291456 | tf_op jit(solution)/shard_map/all_to_all | solution.py:40
  120.1 0.7 fusion
  120.8 0.0 copy-done.3
  120.8 1.1 fusion.3
  121.9 0.0 copy-start.6
  121.9 3.6 %copy.38 = bf16[32,24,16,128]{3,2,1,0:T(8,128)(2,1)S(1)} copy(bf16[32,24,16,128]{3,1,0,2:T(8,128)(2,1)S(1)} %fusion.3) | data formatting | bytes 6291456 | tf_op jit(solution)/shard_map/convert_element_type | solution.py:74
  125.6 0.0 copy-start.1
  125.6 1.7 copy-done.1
  127.2 1.0 fusion.6
  128.2 0.2 copy-done.7
  128.5 6.9 %fusion.10 = bf16[96,8,16,128]{3,1,2,0:T(8,128)(2,1)} fusion(bf16[1,256,2048]{2,1,0:T(8,128)(2,1)S(1)} %copy-done, bf16[96,8,16,128]{3,2,1,0:T(8,128)(2,1)} %bitcast.98, bf16[1,2048,256]{2,1,0:T(8,128)(2,1)S(1)} %copy-done.7, f32[768,256]{1,0:T(8,128)S(1)} %fusion.6), kind=kOutput, calls=%fused_computation.20 | convolution fusion | flops 1613365248 | bytes 9175040 | tf_op jit(solution)/shard_map/dot_general | solution.py:157
  135.4 2.9 %copy.49 = bf16[96,8,16,128]{3,2,1,0:T(8,128)(2,1)S(1)} copy(bf16[96,8,16,128]{3,1,2,0:T(8,128)(2,1)} %fusion.10) | data formatting | bytes 6291456
  138.3 0.8 copy.68
  139.1 43.4 %all_to_all.46 = bf16[16,1,768,128]{3,2,1,0:T(8,128)(2,1)} all-to-all(bf16[16,1,768,128]{3,2,1,0:T(8,128)(2,1)S(1)} %bitcast.96), channel_id=1, replica_groups=mesh['sp'=32,'tp_0'=4,'tp_1'=4] {'tp_0','tp_1'}, dimensions={0} | all-to-all | bytes 6291456 | tf_op jit(solution)/shard_map/all_to_all | solution.py:67
  182.5 3.1 %reduce_sum.64 = bf16[768,128]{1,0:T(8,128)(2,1)} reduce(bf16[16,1,768,128]{3,2,1,0:T(8,128)(2,1)} %all_to_all.46, bf16[]{:T(256)} %constant.87.clone.1), dimensions={0,1}, to_apply=%region_9.10 | reduce | flops 1474560 | bytes 3342338 | tf_op jit(solution)/shard_map/reduce_sum | solution.py:161
  185.5 3.9 %all-to-all-start.4 = ((bf16[32,24,128]{2,1,0:T(8,128)(2,1)}), bf16[32,24,128]{2,1,0:T(8,128)(2,1)S(1)}, u32[]{:S(2)}, u32[]{:S(2)}) async-start(bf16[32,24,128]{2,1,0:T(8,128)(2,1)} %bitcast.17), calls=%async_computation.4 | async-start | bytes 393216 | tf_op jit(solution)/shard_map/all_to_all | solution.py:163
  189.4 0.0 copy-done.4
  189.4 0.1 copy.40
  189.6 19.8 %all-to-all-done.4 = bf16[32,24,128]{2,1,0:T(8,128)(2,1)S(1)} async-done(((bf16[32,24,128]{2,1,0:T(8,128)(2,1)}), bf16[32,24,128]{2,1,0:T(8,128)(2,1)S(1)}, u32[]{:S(2)}, u32[]{:S(2)}) %all-to-all-start.4) | async-done | bytes 196640 | tf_op jit(solution)/shard_map/all_to_all | solution.py:163
  209.4 1.0 gather_fusion.1
  210.5 0.4 multiply_reduce_fusion
  210.9 10.2 %all_to_all.47 = bf16[16,16,128]{2,1,0:T(8,128)(2,1)S(1)} all-to-all(bf16[16,16,128]{2,1,0:T(8,128)(2,1)S(1)} %bitcast.101), channel_id=1, replica_groups=mesh['sp'=32,'tp_0'=4,'tp_1'=4] {'tp_0','tp_1'}, dimensions={0} | all-to-all | bytes 131072 | tf_op jit(solution)/shard_map/all_to_all | solution.py:171
  221.1 0.6 copy_bitcast_fusion.1
  (24 shorter events, 0.2 us)
Async XLA Ops:
  0.0 128.2 %copy-start = (bf16[1,256,2048]{2,1,0:T(8,128)(2,1)S(1)}, bf16[1,256,2048]{2,1,0:T(8,128)(2,1)}, u32[]{:S(2)}) copy-start(bf16[1,256,2048]{2,1,0:T(8,128)(2,1)} %param.23) | copy-start | bytes 3145732
  0.0 14.1 %copy-start.5 = (f32[2]{0:T(128)S(1)}, f32[2]{0:T(128)}, u32[]{:S(2)}) copy-start(f32[2]{0:T(128)} %param.15) | copy-start | bytes 28
  1.1 11.8 %collective-permute-start.1 = (bf16[128,64]{0,1:T(8,128)(2,1)S(1)}, bf16[128,64]{0,1:T(8,128)(2,1)S(1)}, u32[]{:S(2)}, u32[]{:S(2)}) collective-permute-start(bf16[128,64]{0,1:T(8,128)(2,1)S(1)} %slice.21), channel_id=1, source_target_pairs={{0,16},{16,32},{32,48},{48,64},{64,80},{80,96},{96,112},{112,128},... | collective-permute-start | bytes 49160 | tf_op jit(solution)/shard_map/ppermute | solution.py:18
  3.9 10.5 %copy-start.2 = (bf16[128,2048]{1,0:T(8,128)(2,1)S(1)}, bf16[128,2048]{1,0:T(8,128)(2,1)}, u32[]{:S(2)}) copy-start(bf16[128,2048]{1,0:T(8,128)(2,1)} %param.16) | copy-start | bytes 1572868
  3.9 10.2 %collective-permute-start = (bf16[128,64]{0,1:T(8,128)(2,1)S(1)}, bf16[128,64]{0,1:T(8,128)(2,1)S(1)}, u32[]{:S(2)}, u32[]{:S(2)}) collective-permute-start(bf16[128,64]{0,1:T(8,128)(2,1)S(1)} %slice.20), channel_id=1, source_target_pairs={{0,16},{16,32},{32,48},{48,64},{64,80},{80,96},{96,112},{112,128},... | collective-permute-start | bytes 49160 | tf_op jit(solution)/shard_map/ppermute | solution.py:18
  16.2 23.4 %all-to-all-start = ((bf16[16,256,128]{2,1,0:T(8,128)(2,1)}), bf16[16,256,128]{2,1,0:T(8,128)(2,1)S(1)}, u32[]{:S(2)}, u32[]{:S(2)}) async-start(bf16[16,256,128]{2,1,0:T(8,128)(2,1)} %bitcast.94), calls=%async_computation | async-start | bytes 2097152 | tf_op jit(solution)/shard_map/all_to_all | solution.py:28
  120.1 0.7 copy-start.3
  121.9 5.3 %copy-start.6 = (bf16[1,2048,256]{2,1,0:T(8,128)(2,1)S(1)}, bf16[1,2048,256]{2,1,0:T(8,128)(2,1)}, u32[]{:S(2)}) copy-start(bf16[1,2048,256]{2,1,0:T(8,128)(2,1)} %param.21) | copy-start | bytes 3145732
  125.6 1.7 copy-start.1
  127.2 1.2 copy-start.7
  182.5 6.9 %copy-start.4 = (f32[256,2]{0,1:T(2,128)S(1)}, f32[256,2]{0,1:T(2,128)}, u32[]{:S(2)}) copy-start(f32[256,2]{0,1:T(2,128)} %param.20) | copy-start | bytes 6148
  185.5 23.8 %all-to-all-start.4 = ((bf16[32,24,128]{2,1,0:T(8,128)(2,1)}), bf16[32,24,128]{2,1,0:T(8,128)(2,1)S(1)}, u32[]{:S(2)}, u32[]{:S(2)}) async-start(bf16[32,24,128]{2,1,0:T(8,128)(2,1)} %bitcast.17), calls=%async_computation.4 | async-start | bytes 393216 | tf_op jit(solution)/shard_map/all_to_all | solution.py:163
where the time goes:
time: 223 us; the launch traced here: 222 us
  blocking collectives  130 us (58%)
  waiting for transfers between devices  30.6 us (14%)
  local copies, waits for them, and re-layouts  24.5 us (11%)
  starting transfers between devices  17.3 us (8%)
  other arithmetic  9.61 us (4%)
  matrix products  8.91 us (4%)
    all_to_all x1, blocking collectives, exchange_in_pieces(): lax.all_to_all(slab, axis, split_axis=0, concat_axis=0, tiled=True)  43.4 us
    all_to_all x1, blocking collectives, sent_to_all(): return lax.all_to_all(copies, axis, split_axis=0, concat_axis=0, tiled=True)  42.4 us
    all_to_all x1, blocking collectives, per_device(): lax.all_to_all(outgoing, 'sp', split_axis=0, concat_axis=0, tiled=True)  34.4 us
    all_to_all x1, waiting for transfers between devices, per_device(): lax.all_to_all(summed.astype(jnp.bfloat16), 'sp', split_axis=0, concat_ax...  19.8 us
    all_to_all x1, waiting for transfers between devices, sum_at_owner(): lax.all_to_all(pieces, axis, split_axis=0, concat_axis=0, tiled=True)  10.8 us
    all_to_all x1, blocking collectives, per_device(): lax.all_to_all(out_columns, TP, split_axis=0, concat_axis=1, tiled=True)  10.2 us
    all_to_all x1, starting transfers between devices, sum_at_owner(): lax.all_to_all(pieces, axis, split_axis=0, concat_axis=0, tiled=True)  7.48 us
    dot_general x1, matrix products, per_device(): jnp.dot(hidden, down_weight[0], preferred_element_type=jnp.float32)  6.92 us
  transfers between devices with their start and end apart: 4, of which 2 were waited for; matrix products, arithmetic and copies ran while one was open for 5% of the time, Pallas kernels for 0%

commit v1 on v0

--- a/solution.py
+++ b/solution.py
@@ -3,6 +3,7 @@
 from jax import lax
 from jax.sharding import Mesh
 from jax.sharding import PartitionSpec as P
+from jax.lax import all_to_all, psum
 
 HEAD_DIM = 64
 REP = 8
@@ -168,7 +169,9 @@
     chosen = returned_flat[targets] * pair_weights[:, None]
     moe_columns = jnp.sum(chosen.reshape(tok_count, top_count, chosen.shape[1]), axis=1)
     out_columns = (columns.astype(jnp.float32) + moe_columns).astype(jnp.bfloat16)
-    return lax.all_to_all(out_columns, TP, split_axis=0, concat_axis=1, tiled=True)
+    return jnp.concatenate(
+        all_to_all(jnp.stack(jnp.split(out_columns, psum(1, TP), axis=0), axis=0), TP, 0, 0), axis=1
+    )
 
 
 def solution(mesh):

time: 223 us -> 223 us (level)
    unnamed x22 -> x37, local copies, waits for them, and re-layouts: 6.88 us -> 7.01 us
where the time goes in v1:
time: 223 us; the launch traced here: 222 us
  blocking collectives  130 us (58%)
  waiting for transfers between devices  30.6 us (14%)
  local copies, waits for them, and re-layouts  24.6 us (11%)
  starting transfers between devices  17.3 us (8%)
  other arithmetic  9.61 us (4%)
  matrix products  8.91 us (4%)
    all_to_all x1, blocking collectives, exchange_in_pieces(): lax.all_to_all(slab, axis, split_axis=0, concat_axis=0, tiled=True)  43.4 us
    all_to_all x1, blocking collectives, sent_to_all(): return lax.all_to_all(copies, axis, split_axis=0, concat_axis=0, tiled=True)  42.4 us
    all_to_all x1, blocking collectives, per_device(): lax.all_to_all(outgoing, 'sp', split_axis=0, concat_axis=0, tiled=True)  34.4 us
    all_to_all x1, waiting for transfers between devices, per_device(): lax.all_to_all(summed.astype(jnp.bfloat16), 'sp', split_axis=0, concat_ax...  19.8 us
    all_to_all x1, waiting for transfers between devices, sum_at_owner(): lax.all_to_all(pieces, axis, split_axis=0, concat_axis=0, tiled=True)  10.8 us
    all_to_all x1, blocking collectives, per_device(): all_to_all(jnp.stack(jnp.split(out_columns, psum(1, TP), axis=0), axis=0)...  10.2 us
    all_to_all x1, starting transfers between devices, sum_at_owner(): lax.all_to_all(pieces, axis, split_axis=0, concat_axis=0, tiled=True)  7.48 us
    unnamed x37, local copies, waits for them, and re-layouts  7.01 us
  transfers between devices with their start and end apart: 4, of which 2 were waited for; matrix products, arithmetic and copies ran while one was open for 5% of the time, Pallas kernels for 0%

profile of v1, /device:TPU:2, one launch (start us, length us, event | category | flops | bytes accessed | tf_op | source)
XLA Modules:
  0.0 221.9 jit_solution(13956166881251069340)
XLA Ops:
  0.0 0.0 copy-start
  0.0 1.0 constant_dynamic-slice_fusion
  1.0 0.1 copy.43
  1.1 1.7 collective-permute-start.1
  2.9 0.9 constant_dynamic-slice_fusion.1
  3.8 0.1 copy.42
  3.9 0.0 copy-start.2
  3.9 4.2 %collective-permute-start = (bf16[128,64]{0,1:T(8,128)(2,1)S(1)}, bf16[128,64]{0,1:T(8,128)(2,1)S(1)}, u32[]{:S(2)}, u32[]{:S(2)}) collective-permute-start(bf16[128,64]{0,1:T(8,128)(2,1)S(1)} %slice.20), channel_id=1, source_target_pairs={{0,16},{16,32},{32,48},{48,64},{64,80},{80,96},{96,112},{112,128},... | collective-permute-start | bytes 49160 | tf_op jit(solution)/shard_map/ppermute | solution.py:19
  8.2 0.8 copy.34
  9.1 0.7 broadcast_multiply_fusion
  9.7 0.1 eq.29
  9.9 1.2 reduce-window.6
  11.1 0.2 fusion.30
  11.3 0.2 slice_reduce_fusion
  11.5 0.1 eq.25
  11.6 0.9 copy.30
  12.6 0.1 copy.33
  12.7 0.1 mul.101
  12.9 0.0 collective-permute-done.1
  12.9 0.3 fusion.49
  13.2 0.7 broadcast_maximum_fusion
  13.9 0.1 fusion.27
  14.1 0.0 copy-done.5
  14.1 0.1 exponential_add_fusion
  14.1 0.0 collective-permute-done
  14.2 0.3 convolution_convert_fusion.2
  14.4 0.0 copy-done.2
  14.4 0.4 fusion.11
  14.9 1.3 copy.68
  16.2 7.5 %all-to-all-start = ((bf16[16,256,128]{2,1,0:T(8,128)(2,1)}), bf16[16,256,128]{2,1,0:T(8,128)(2,1)S(1)}, u32[]{:S(2)}, u32[]{:S(2)}) async-start(bf16[16,256,128]{2,1,0:T(8,128)(2,1)} %bitcast.157), calls=%async_computation | async-start | bytes 2097152 | tf_op jit(solution)/shard_map/all_to_all | solution.py:29
  23.6 0.1 fusion.33
  23.8 2.4 %scatter_custom_fusion.1 = s32[768]{0:T(1024)S(1)} fusion(s32[512]{0:T(512)S(1)} %bitcast.167, s32[512]{0:T(512)S(1)} %add_select_fusion, s32[]{:T(128)} %constant.30.clone.1), kind=kCustom, calls=%fused_computation.104 | custom fusion | bytes 3076 | tf_op jit(solution)/shard_map/scatter | solution.py:86
  26.2 2.4 %scatter_custom_fusion = s32[768]{0:T(1024)S(1)} fusion(s32[512]{0:T(512)S(1)} %bitcast.168, s32[512]{0:T(512)S(1)} %broadcast.197, s32[]{:T(128)} %constant.30.clone.1), kind=kCustom, calls=%fused_computation.107 | custom fusion | bytes 3076 | tf_op jit(solution)/shard_map/scatter | solution.py:87
  28.7 0.1 broadcast_in_dim.51
  28.8 10.8 %all-to-all-done = bf16[16,256,128]{2,1,0:T(8,128)(2,1)S(1)} async-done(((bf16[16,256,128]{2,1,0:T(8,128)(2,1)}), bf16[16,256,128]{2,1,0:T(8,128)(2,1)S(1)}, u32[]{:S(2)}, u32[]{:S(2)}) %all-to-all-start) | async-done | bytes 1048608 | tf_op jit(solution)/shard_map/all_to_all | solution.py:29
  39.6 0.1 convert_reduce_fusion
  39.7 0.9 add_convert_fusion.1
  40.6 1.9 gather_fusion
  42.5 0.2 broadcast_select_fusion
  42.7 34.4 %all_to_all.30 = bf16[32,24,128]{2,1,0:T(8,128)(2,1)S(1)} all-to-all(bf16[32,24,128]{2,1,0:T(8,128)(2,1)S(1)} %broadcast_select_fusion), channel_id=1, replica_groups=mesh['sp'=32,'tp_0'=4,'tp_1'=4] {'sp'}, dimensions={0} | all-to-all | bytes 393216 | tf_op jit(solution)/shard_map/all_to_all | solution.py:150
  77.1 0.6 broadcast_in_dim.55
  77.7 42.4 %all_to_all.31 = bf16[16,32,24,128]{3,2,1,0:T(8,128)(2,1)S(1)} all-to-all(bf16[16,32,24,128]{3,2,1,0:T(8,128)(2,1)S(1)} %broadcast_in_dim.55), channel_id=1, replica_groups=mesh['sp'=32,'tp_0'=4,'tp_1'=4] {'tp_0','tp_1'}, dimensions={0} | all-to-all | bytes 6291456 | tf_op jit(solution)/shard_map/all_to_all | solution.py:41
  120.1 0.7 fusion
  120.8 0.0 copy-done.3
  120.8 1.1 fusion.3
  121.9 0.0 copy-start.6
  121.9 3.6 %copy.37 = bf16[32,24,16,128]{3,2,1,0:T(8,128)(2,1)S(1)} copy(bf16[32,24,16,128]{3,1,0,2:T(8,128)(2,1)S(1)} %fusion.3) | data formatting | bytes 6291456 | tf_op jit(solution)/shard_map/convert_element_type | solution.py:75
  125.6 0.0 copy-start.1
  125.6 1.7 copy-done.1
  127.2 1.0 fusion.6
  128.2 0.2 copy-done.7
  128.5 6.9 %fusion.10 = bf16[96,8,16,128]{3,1,2,0:T(8,128)(2,1)} fusion(bf16[1,256,2048]{2,1,0:T(8,128)(2,1)S(1)} %copy-done, bf16[96,8,16,128]{3,2,1,0:T(8,128)(2,1)} %bitcast.161, bf16[1,2048,256]{2,1,0:T(8,128)(2,1)S(1)} %copy-done.7, f32[768,256]{1,0:T(8,128)S(1)} %fusion.6), kind=kOutput, calls=%fused_computation.20 | convolution fusion | flops 1613365248 | bytes 9175040 | tf_op jit(solution)/shard_map/dot_general | solution.py:158
  135.4 2.9 %copy.48 = bf16[96,8,16,128]{3,2,1,0:T(8,128)(2,1)S(1)} copy(bf16[96,8,16,128]{3,1,2,0:T(8,128)(2,1)} %fusion.10) | data formatting | bytes 6291456
  138.3 0.8 copy.67
  139.1 43.4 %all_to_all.32 = bf16[16,1,768,128]{3,2,1,0:T(8,128)(2,1)} all-to-all(bf16[16,1,768,128]{3,2,1,0:T(8,128)(2,1)S(1)} %bitcast.159), channel_id=1, replica_groups=mesh['sp'=32,'tp_0'=4,'tp_1'=4] {'tp_0','tp_1'}, dimensions={0} | all-to-all | bytes 6291456 | tf_op jit(solution)/shard_map/all_to_all | solution.py:68
  182.5 3.1 %reduce_sum.64 = bf16[768,128]{1,0:T(8,128)(2,1)} reduce(bf16[16,1,768,128]{3,2,1,0:T(8,128)(2,1)} %all_to_all.32, bf16[]{:T(256)} %constant.87.clone.1), dimensions={0,1}, to_apply=%region_9.10 | reduce | flops 1474560 | bytes 3342338 | tf_op jit(solution)/shard_map/reduce_sum | solution.py:162
  185.5 3.9 %all-to-all-start.4 = ((bf16[32,24,128]{2,1,0:T(8,128)(2,1)}), bf16[32,24,128]{2,1,0:T(8,128)(2,1)S(1)}, u32[]{:S(2)}, u32[]{:S(2)}) async-start(bf16[32,24,128]{2,1,0:T(8,128)(2,1)} %bitcast.17), calls=%async_computation.4 | async-start | bytes 393216 | tf_op jit(solution)/shard_map/all_to_all | solution.py:164
  189.4 0.0 copy-done.4
  189.4 0.1 copy.39
  189.6 19.8 %all-to-all-done.4 = bf16[32,24,128]{2,1,0:T(8,128)(2,1)S(1)} async-done(((bf16[32,24,128]{2,1,0:T(8,128)(2,1)}), bf16[32,24,128]{2,1,0:T(8,128)(2,1)S(1)}, u32[]{:S(2)}, u32[]{:S(2)}) %all-to-all-start.4) | async-done | bytes 196640 | tf_op jit(solution)/shard_map/all_to_all | solution.py:164
  209.4 1.0 gather_fusion.1
  210.5 0.4 multiply_reduce_fusion
  211.1 10.2 %all_to_all.33 = bf16[16,16,128]{2,1,0:T(8,128)(2,1)S(1)} all-to-all(bf16[16,16,128]{2,1,0:T(8,128)(2,1)S(1)} %constant_dynamic-update-slice_fusion), channel_id=1, replica_groups=mesh['sp'=32,'tp_0'=4,'tp_1'=4] {'tp_0','tp_1'}, dimensions={0} | all-to-all | bytes 131072 | tf_op jit(solution)/shard_map/all_to_all | solution.py:173
  221.3 0.6 copy_bitcast_fusion.1
  (40 shorter events, 0.3 us)
Async XLA Ops:
  0.0 128.2 %copy-start = (bf16[1,256,2048]{2,1,0:T(8,128)(2,1)S(1)}, bf16[1,256,2048]{2,1,0:T(8,128)(2,1)}, u32[]{:S(2)}) copy-start(bf16[1,256,2048]{2,1,0:T(8,128)(2,1)} %param.23) | copy-start | bytes 3145732
  0.0 14.1 %copy-start.5 = (f32[2]{0:T(128)S(1)}, f32[2]{0:T(128)}, u32[]{:S(2)}) copy-start(f32[2]{0:T(128)} %param.15) | copy-start | bytes 28
  1.1 11.8 %collective-permute-start.1 = (bf16[128,64]{0,1:T(8,128)(2,1)S(1)}, bf16[128,64]{0,1:T(8,128)(2,1)S(1)}, u32[]{:S(2)}, u32[]{:S(2)}) collective-permute-start(bf16[128,64]{0,1:T(8,128)(2,1)S(1)} %slice.21), channel_id=1, source_target_pairs={{0,16},{16,32},{32,48},{48,64},{64,80},{80,96},{96,112},{112,128},... | collective-permute-start | bytes 49160 | tf_op jit(solution)/shard_map/ppermute | solution.py:19
  3.9 10.5 %copy-start.2 = (bf16[128,2048]{1,0:T(8,128)(2,1)S(1)}, bf16[128,2048]{1,0:T(8,128)(2,1)}, u32[]{:S(2)}) copy-start(bf16[128,2048]{1,0:T(8,128)(2,1)} %param.16) | copy-start | bytes 1572868
  3.9 10.2 %collective-permute-start = (bf16[128,64]{0,1:T(8,128)(2,1)S(1)}, bf16[128,64]{0,1:T(8,128)(2,1)S(1)}, u32[]{:S(2)}, u32[]{:S(2)}) collective-permute-start(bf16[128,64]{0,1:T(8,128)(2,1)S(1)} %slice.20), channel_id=1, source_target_pairs={{0,16},{16,32},{32,48},{48,64},{64,80},{80,96},{96,112},{112,128},... | collective-permute-start | bytes 49160 | tf_op jit(solution)/shard_map/ppermute | solution.py:19
  16.2 23.4 %all-to-all-start = ((bf16[16,256,128]{2,1,0:T(8,128)(2,1)}), bf16[16,256,128]{2,1,0:T(8,128)(2,1)S(1)}, u32[]{:S(2)}, u32[]{:S(2)}) async-start(bf16[16,256,128]{2,1,0:T(8,128)(2,1)} %bitcast.157), calls=%async_computation | async-start | bytes 2097152 | tf_op jit(solution)/shard_map/all_to_all | solution.py:29
  120.1 0.7 copy-start.3
  121.9 5.3 %copy-start.6 = (bf16[1,2048,256]{2,1,0:T(8,128)(2,1)S(1)}, bf16[1,2048,256]{2,1,0:T(8,128)(2,1)}, u32[]{:S(2)}) copy-start(bf16[1,2048,256]{2,1,0:T(8,128)(2,1)} %param.21) | copy-start | bytes 3145732
  125.6 1.7 copy-start.1
  127.2 1.2 copy-start.7
  182.5 6.9 %copy-start.4 = (f32[256,2]{0,1:T(2,128)S(1)}, f32[256,2]{0,1:T(2,128)}, u32[]{:S(2)}) copy-start(f32[256,2]{0,1:T(2,128)} %param.20) | copy-start | bytes 6148
  185.5 23.8 %all-to-all-start.4 = ((bf16[32,24,128]{2,1,0:T(8,128)(2,1)}), bf16[32,24,128]{2,1,0:T(8,128)(2,1)S(1)}, u32[]{:S(2)}, u32[]{:S(2)}) async-start(bf16[32,24,128]{2,1,0:T(8,128)(2,1)} %bitcast.17), calls=%async_computation.4 | async-start | bytes 393216 | tf_op jit(solution)/shard_map/all_to_all | solution.py:164
